TPU v7x, 32 devices: a whole 2x2x4 slice. The times are simulated.
32 devices in a mesh: sp: 4 (over y, x), tp: 8 (over z, core).
Axes of the slice: x: 2, y: 2, z: 4, core: 2. Of those that a mesh axis runs over, the one named last changes fastest.
Arguments:
- skip_stream_entry: bfloat16 [2048, 2048], P(('sp', 'tp')), may hold values from -6 to 6
- result_switch_mapped: bfloat16 [2048, 4096], P('sp', 'tp'), may hold values from -6 to 6
- channel_feed_mapped: bfloat16 [2048, 4096], P('sp', 'tp'), may hold values from -6 to 6
- write_coefficient_mapped: bfloat16 [2048, 2048], P('sp', 'tp'), may hold values from -6 to 6
- emission_coefficient_mapped: bfloat16 [2048, 2048], P('sp', 'tp'), may hold values from -6 to 6
- channel_feed_taps: bfloat16 [5, 4096], P(None, 'tp'), may hold values from -2.5 to 2.5
- write_coefficient_taps: bfloat16 [5, 2048], P(None, 'tp'), may hold values from -2.5 to 2.5
- emission_coefficient_taps: bfloat16 [5, 2048], P(None, 'tp'), may hold values from -2.5 to 2.5
- raw_increments: bfloat16 [2, 64, 2048], P(None, 'tp', 'sp'), may hold values from -6 to 6
- channel_log_fade_speed: float32 [2, 64], P(None, 'tp'), may hold values from -20 to 0
- extra_log_fade: float32 [2, 64, 2048], P(None, 'tp', 'sp'), may hold values from -1 to 0
- cluster_scaling_factor: float32 [4096], P('tp'), may hold values from 0.1 to 1.9
- blend_result_matrix: bfloat16 [4096, 2048], P('tp'), may hold values from -0.09375 to 0.09375
- routing_scaling_factor: float32 [2048], replicated, may hold values from 0.1 to 1.9
- specialist_switch_matrix: bfloat16 [8, 2048, 4096], P('sp', None, 'tp'), may hold values from -0.125 to 0.125
- specialist_widen_matrix: bfloat16 [8, 2048, 4096], P('sp', None, 'tp'), may hold values from -0.125 to 0.125
- specialist_contract_matrix: bfloat16 [8, 4096, 2048], P('sp', 'tp'), may hold values from -0.1875 to 0.1875
- picked_specialists: int32 [2048, 2], P(('sp', 'tp')), may hold values from 0 to 7, all different within a row; in each aligned block of 64 rows (0 to 63, 64 to 127, ...) at most 24 rows name the same one
- router_affinities: float32 [2048, 2], P(('sp', 'tp')), may hold values from 0.1 to 1
Outputs:
- result: bfloat16 [2048, 2048], P(('sp', 'tp'))
Inputs may be any that keep to these rules, and one draw needn't show every extreme that they name: `picked_specialists`: each row names 2 different experts. Within the rows of one device (aligned blocks of 64 rows) no expert is named more than 24 times, a bound that some block reaches.
All inputs are finite; a program needn't handle non-finite values.
Results may differ from a plain program's by a relative error of at most 0.02.
Values may be sent and summed in bfloat16 or wider, within the bound.
No kernel may reach another device: no remote copies, remote signals or barrier semaphores. Data moves between devices by JAX's collectives and lax.ppermute only.
A program may use at most 64 MiB of HBM per device.

v0:
```python
import jax
import jax.numpy as jnp
from jax import lax
from jax.sharding import PartitionSpec as P

WIDTH = 2048
HEAD_DIM = 64
GROUPS = 16
STATE = 128
CONV_W = 5
BLOCK = 128
TOP = 2
INNER = 4096


EPSILON = 1e-06
HIGHEST_MODE = lax.Precision.HIGHEST


def with_halo(block, sides, width):
    for axis, dim in sides:
        count = lax.axis_size(axis)
        forward = [(i, i + 1) for i in range(count - 1)]
        backward = [(target, source) for source, target in forward]
        low = lax.ppermute(
            lax.slice_in_dim(block, block.shape[dim] - width, None, axis=dim), axis, forward
        )
        high = lax.ppermute(lax.slice_in_dim(block, 0, width, axis=dim), axis, backward)
        block = jnp.concatenate([low, block, high], axis=dim)
    return block


def prefix(shard, axis, combine, identity, reverse):
    peers, here = (lax.axis_size(axis), lax.axis_index(axis))
    everything = jax.tree.map(
        lambda part, kind: lax.all_gather(part.astype(kind), axis),
        shard,
        (jnp.bfloat16, jnp.bfloat16),
    )
    start = jax.tree.map(
        lambda part, zero: jnp.broadcast_to(jnp.asarray(zero, part.dtype), part.shape),
        shard,
        identity,
    )

    def hop(k, before):
        at = peers - 1 - k if reverse else k
        reached = at > here if reverse else at < here
        new = combine(
            before, jax.tree.map(lambda part, own: part[at].astype(own.dtype), everything, shard)
        )
        return jax.tree.map(lambda a, b: jnp.where(reached, a, b), new, before)

    return lax.fori_loop(0, peers, hop, start)


def centred_conv(padded, weights, series_count):
    summed = jnp.zeros((series_count, padded.shape[1]), jnp.float32)
    for offset in range(weights.shape[0]):
        summed = summed + weights[offset].astype(jnp.float32) * padded[
            offset : offset + series_count
        ].astype(jnp.float32)
    return jax.nn.silu(summed)


def local_sweep(inputs, entry_state, readout_state, log_fade_factor, softplus_increment):
    seq_len = inputs.shape[0]
    blocks = seq_len // BLOCK
    heads_here = log_fade_factor.shape[0]
    groups_here = entry_state.shape[1] // STATE
    per_group = heads_here // groups_here
    values = inputs.reshape(blocks, BLOCK, groups_here, per_group, HEAD_DIM)
    b_blocks = entry_state.reshape(blocks, BLOCK, groups_here, STATE)
    c_blocks = readout_state.reshape(blocks, BLOCK, groups_here, STATE)
    decay_blocks = log_fade_factor.reshape(groups_here, per_group, blocks, BLOCK)
    step_blocks = softplus_increment.reshape(groups_here, per_group, blocks, BLOCK)
    cumulative = jnp.cumsum(decay_blocks, axis=-1)
    group_inner = jnp.einsum("bign,bjgn->gbij", c_blocks, b_blocks, precision=HIGHEST_MODE)
    spread = cumulative[..., :, None] - cumulative[..., None, :]
    lower_tri = jnp.arange(BLOCK)[:, None] >= jnp.arange(BLOCK)[None, :]
    mixing = (
        jnp.exp(jnp.where(lower_tri, spread, -jnp.inf))
        * step_blocks[..., None, :]
        * group_inner[:, None]
    )
    within = jnp.einsum("gkbij,bjgkp->bigkp", mixing, values, precision=HIGHEST_MODE)
    to_end = jnp.exp(cumulative[..., -1:] - cumulative) * step_blocks
    block_states = jnp.einsum(
        "gkbj,bjgkp,bjgn->bgkpn", to_end, values, b_blocks, precision=HIGHEST_MODE
    )
    block_decay = cumulative[..., -1]

    def advance(carried, pieces):
        state_piece, decay_piece = pieces
        return (carried * jnp.exp(decay_piece)[..., None, None] + state_piece, carried)

    zero_state = jnp.zeros((groups_here, per_group, HEAD_DIM, STATE), jnp.float32)
    final_state, entering = lax.scan(
        advance, zero_state, (block_states, jnp.moveaxis(block_decay, -1, 0))
    )
    before = jnp.cumsum(block_decay, axis=-1) - block_decay
    return (
        (within, entering, cumulative, before, c_blocks),
        (jnp.sum(block_decay, axis=-1), final_state),
    )


def finish_sweep(parts, carried):
    within, entering, cumulative, before, c_blocks = parts
    entering = entering + carried[None] * jnp.exp(jnp.moveaxis(before, -1, 0))[..., None, None]
    readout = jnp.einsum("bign,bgkpn->bigkp", c_blocks, entering, precision=HIGHEST_MODE)
    readout = readout * jnp.exp(jnp.transpose(cumulative, (2, 3, 0, 1)))[..., None]
    combined = within + readout
    return combined.reshape(combined.shape[0] * combined.shape[1], -1)


def blend_parts_list(
    channel_feed_bordered,
    write_coefficient_bordered,
    emission_coefficient_bordered,
    channel_feed_taps,
    write_coefficient_taps,
    emission_coefficient_taps,
    raw_increments,
    channel_log_fade_speed,
    extra_log_fade,
    series_count,
):
    inputs = centred_conv(channel_feed_bordered, channel_feed_taps, series_count)
    entry_state = centred_conv(write_coefficient_bordered, write_coefficient_taps, series_count)
    readout_state = centred_conv(
        emission_coefficient_bordered, emission_coefficient_taps, series_count
    )
    softplus_increment = jax.nn.softplus(raw_increments.astype(jnp.float32))
    log_fade_factor = (
        -softplus_increment * jnp.exp(channel_log_fade_speed)[..., None] + extra_log_fade
    )
    onward_pass = local_sweep(
        inputs, entry_state, readout_state, log_fade_factor[0], softplus_increment[0]
    )
    backward_pass = local_sweep(
        jnp.flip(inputs, 0),
        jnp.flip(entry_state, 0),
        jnp.flip(readout_state, 0),
        jnp.flip(log_fade_factor[1], -1),
        jnp.flip(softplus_increment[1], -1),
    )
    return (onward_pass, backward_pass)


def gated_norm(mixed_sum, result_switch_mapped, cluster_scaling_factor):
    gated = mixed_sum * jax.nn.silu(result_switch_mapped.astype(jnp.float32))
    grouped = gated.reshape(gated.shape[0], -1, INNER // GROUPS)
    normalized = grouped * lax.rsqrt(jnp.mean(grouped * grouped, axis=-1, keepdims=True) + EPSILON)
    return (normalized.reshape(gated.shape) * cluster_scaling_factor).astype(jnp.bfloat16)


def rms_scale(stream, gain):
    values = stream.astype(jnp.float32)
    return (
        values * lax.rsqrt(jnp.mean(values * values, axis=-1, keepdims=True) + EPSILON) * gain
    ).astype(jnp.bfloat16)


def link_states(former, latter):
    former_total, former_state = former
    latter_total, latter_state = latter
    return (
        former_total + latter_total,
        former_state * jnp.exp(latter_total)[..., None, None] + latter_state,
    )


def per_device(
    skip_stream_entry,
    result_switch_mapped,
    channel_feed_mapped,
    write_coefficient_mapped,
    emission_coefficient_mapped,
    channel_feed_taps,
    write_coefficient_taps,
    emission_coefficient_taps,
    raw_increments,
    channel_log_fade_speed,
    extra_log_fade,
    cluster_scaling_factor,
    blend_result_matrix,
    routing_scaling_factor,
    specialist_switch_matrix,
    specialist_widen_matrix,
    specialist_contract_matrix,
    picked_specialists,
    router_affinities,
):
    series_count = channel_feed_mapped.shape[0]
    rim_width = CONV_W // 2
    sources = (channel_feed_mapped, write_coefficient_mapped, emission_coefficient_mapped)
    edges = jnp.concatenate(
        [jnp.concatenate([source[:rim_width], source[-rim_width:]], 0) for source in sources], 1
    )
    rimmed = with_halo(edges, (("sp", 0),), rim_width)
    padded_list = []
    column_start = 0
    for source in sources:
        width_here = source.shape[1]
        upper_rim = rimmed[:rim_width, column_start : column_start + width_here]
        lower_rim = rimmed[-rim_width:, column_start : column_start + width_here]
        padded_list.append(jnp.concatenate([upper_rim, source, lower_rim], 0))
        column_start = column_start + width_here
    onward_pass, backward_pass = blend_parts_list(
        padded_list[0],
        padded_list[1],
        padded_list[2],
        channel_feed_taps,
        write_coefficient_taps,
        emission_coefficient_taps,
        raw_increments,
        channel_log_fade_speed,
        extra_log_fade,
        series_count,
    )
    fwd_total, fwd_final = onward_pass[1]
    bwd_total, bwd_final = backward_pass[1]
    identity_pair = (jnp.zeros_like(fwd_total), jnp.zeros_like(fwd_final))
    carried_fwd = prefix((fwd_total, fwd_final), "sp", link_states, identity_pair, False)[1]
    carried_bwd = prefix((bwd_total, bwd_final), "sp", link_states, identity_pair, True)[1]
    mixed_sum = finish_sweep(onward_pass[0], carried_fwd) + jnp.flip(
        finish_sweep(backward_pass[0], carried_bwd), 0
    )
    mixed_rows = gated_norm(mixed_sum, result_switch_mapped, cluster_scaling_factor)
    rows_here = skip_stream_entry.shape[0]
    projected = lax.psum_scatter(
        jnp.dot(mixed_rows, blend_result_matrix, preferred_element_type=jnp.float32).astype(
            jnp.bfloat16
        ),
        "tp",
        scatter_dimension=0,
        tiled=True,
    ).astype(jnp.float32)
    after_mixer = (skip_stream_entry.astype(jnp.float32) + projected).astype(jnp.bfloat16)
    normed = rms_scale(after_mixer, routing_scaling_factor)
    experts_here = specialist_switch_matrix.shape[0]
    expert_count = experts_here * lax.axis_size("sp")
    capacity = max(2, 3 * TOP * rows_here // (2 * expert_count))
    slot_total = capacity * expert_count
    flat_routes = picked_specialists.reshape(-1)
    one_hot = (flat_routes[:, None] == jnp.arange(expert_count, dtype=jnp.int32)[None, :]).astype(
        jnp.int32
    )
    earlier_count = jnp.cumsum(one_hot, axis=0) - one_hot
    slot_rank = jnp.sum(earlier_count * one_hot, axis=1)
    position = slot_rank * expert_count + flat_routes
    slot_match = (position[:, None] == jnp.arange(slot_total, dtype=jnp.int32)[None, :]).astype(
        jnp.bfloat16
    )
    buffer = jnp.einsum(
        "rks,rd->sd",
        slot_match.reshape(rows_here, TOP, slot_total),
        normed,
        preferred_element_type=jnp.float32,
    ).astype(jnp.bfloat16)
    buffer = buffer.reshape(capacity, expert_count, WIDTH)
    received = lax.all_to_all(buffer, "sp", split_axis=1, concat_axis=0, tiled=True)
    data_block = lax.all_gather(received, "tp", axis=0, tiled=True)
    gate_part = jnp.einsum(
        "red,edf->ref", data_block, specialist_switch_matrix, preferred_element_type=jnp.float32
    )
    up_part = jnp.einsum(
        "red,edf->ref", data_block, specialist_widen_matrix, preferred_element_type=jnp.float32
    )
    hidden = (jax.nn.silu(gate_part) * up_part).astype(jnp.bfloat16)
    expert_out = lax.psum_scatter(
        jnp.einsum(
            "ref,efd->red", hidden, specialist_contract_matrix, preferred_element_type=jnp.float32
        ).astype(jnp.bfloat16),
        "tp",
        scatter_dimension=0,
        tiled=True,
    )
    returned = lax.all_to_all(expert_out, "sp", split_axis=0, concat_axis=1, tiled=True)
    picked = jnp.dot(
        slot_match, returned.reshape(slot_total, WIDTH), preferred_element_type=jnp.float32
    )
    weights = router_affinities / jnp.sum(router_affinities, axis=-1, keepdims=True)
    mixture = jnp.sum(weights[..., None] * picked.reshape(rows_here, TOP, WIDTH), axis=1)
    return (after_mixer.astype(jnp.float32) + mixture).astype(jnp.bfloat16)


def solution(mesh):
    in_specs = (
        P(("sp", "tp"), None),
        P("sp", "tp"),
        P("sp", "tp"),
        P("sp", "tp"),
        P("sp", "tp"),
        P(None, "tp"),
        P(None, "tp"),
        P(None, "tp"),
        P(None, "tp", "sp"),
        P(None, "tp"),
        P(None, "tp", "sp"),
        P("tp"),
        P("tp", None),
        P(),
        P("sp", None, "tp"),
        P("sp", None, "tp"),
        P("sp", "tp", None),
        P(("sp", "tp"), None),
        P(("sp", "tp"), None),
    )
    out_specs = P(("sp", "tp"), None)
    return jax.shard_map(
        per_device, mesh=mesh, in_specs=in_specs, out_specs=out_specs, check_vma=False
    )
```

profile of v0, /device:TPU:0, one launch (start us, length us, event | category | flops | bytes accessed | tf_op | source)
XLA Modules:
  0.0 437.1 jit_solution(5094532863845228223)
XLA Ops:
  9.1 5.6 %collective-permute-start = (bf16[2,1024]{0,1:T(8,128)(2,1)}, bf16[2,1024]{0,1:T(8,128)(2,1)}, u32[]{:S(2)}, u32[]{:S(2)}) collective-permute-start(bf16[2,1024]{0,1:T(8,128)(2,1)} %copy.175), channel_id=1, source_target_pairs={{0,8},{8,16},{16,24},{1,9},{9,17},{17,25},{2,10},{10,18},{18,26},{... | collective-permute-start | bytes 12296 | tf_op jit(solution)/shard_map/ppermute | solution.py:25
  30.8 9.6 %all-gather.4 = bf16[4,2,4]{2,1,0:T(2,128)(2,1)} all-gather(bf16[1,2,4]{2,1,0:T(2,128)(2,1)S(1)} %bitcast.210), channel_id=2, replica_groups=mesh['sp'=4,'tp'=8] {'sp'}, dimensions={0}, use_global_device_ids=true | all-gather | bytes 80 | tf_op jit(solution)/shard_map/all_gather | solution.py:36
  40.5 8.3 %all-gather.5 = bf16[4,2,4]{2,1,0:T(2,128)(2,1)} all-gather(bf16[1,2,4]{2,1,0:T(2,128)(2,1)S(1)} %bitcast.211), channel_id=4, replica_groups=mesh['sp'=4,'tp'=8] {'sp'}, dimensions={0}, use_global_device_ids=true | all-gather | bytes 80 | tf_op jit(solution)/shard_map/all_gather | solution.py:36
  66.7 4.7 %rev.24 = f32[512,256]{1,0:T(8,128)} reverse(f32[512,256]{1,0:T(8,128)} %divide_multiply_fusion.2), dimensions={0} | reverse | bytes 1048576 | tf_op jit(solution)/shard_map/jit(_flip)/rev | solution.py:144
  76.8 4.7 %rev.25 = f32[512,256]{1,0:T(8,128)} reverse(f32[512,256]{1,0:T(8,128)} %divide_multiply_fusion.1), dimensions={0} | reverse | bytes 1048576 | tf_op jit(solution)/shard_map/jit(_flip)/rev | solution.py:143
  83.4 4.7 %divide_multiply_fusion = f32[512,512]{0,1:T(8,128)} fusion(bf16[512,512]{0,1:T(8,128)(2,1)} %copy.176, bf16[2,512]{0,1:T(8,128)(2,1)S(1)} %slice.207, bf16[2,512]{0,1:T(8,128)(2,1)S(1)} %slice.203, f32[512]{0:T(512)S(1)} %bitcast.198, f32[512]{0:T(512)S(1)} %bitcast.199, f32[512]{0:T(512)S(1)} %bitcast.196, f32[512]{0:T(512)S(1)} %bitcast.197, ...), kind=kLoop, calls=%fused_computation.78 | loop fusion | flops 7864320 | bytes 1587200 | tf_op jit(solution)/shard_map/jit(silu)/mul | solution.py:63
  90.7 9.4 %rev.21 = f32[512,512]{0,1:T(8,128)} reverse(f32[512,512]{0,1:T(8,128)} %divide_multiply_fusion), dimensions={0} | reverse | bytes 2097152 | tf_op jit(solution)/shard_map/jit(_flip)/rev | solution.py:142
  108.0 9.8 %while.56 = (s32[]{:T(128)}, f32[2,4,64,128]{3,2,1,0:T(8,128)S(1)}, f32[4,2,4,64,128]{4,3,2,1,0:T(8,128)}, f32[4,2,4]{2,1,0:T(2,128)}, f32[4,2,4,64,128]{4,3,2,1,0:T(8,128)}, /*index=5*/s32[]{:T(128)}, s32[]{:T(128)}) while((s32[]{:T(128)}, f32[2,4,64,128]{3,2,1,0:T(8,128)S(1)}, f32[4,2,4,64,128]{4,3,2,1,0:T(8,128)}, ...), condition=%wide.region_2.3_spmd.clone, body=%wide.region_1.2_spmd.clone.sunk | while | flops 262147 | bytes 1311424 | solution.py:98
  117.8 10.1 %all-gather.1 = bf16[8,4,64,128]{3,2,1,0:T(8,128)(2,1)} all-gather(bf16[2,4,64,128]{3,2,1,0:T(8,128)(2,1)S(1)} %convert_element_type.229), channel_id=3, replica_groups=mesh['sp'=4,'tp'=8] {'sp'}, dimensions={0}, use_global_device_ids=true | all-gather | bytes 655360 | tf_op jit(solution)/shard_map/all_gather | solution.py:36
  127.9 6.8 %while.57 = (s32[]{:T(128)}, f32[2,4,64,128]{3,2,1,0:T(8,128)S(1)}, s32[]{:T(128)}, bf16[4,2,4]{2,1,0:T(2,128)(2,1)}, bf16[4,2,4,64,128]{4,3,2,1,0:T(8,128)(2,1)}, /*index=5*/s32[]{:T(128)}, s32[]{:T(128)}) while((s32[]{:T(128)}, f32[2,4,64,128]{3,2,1,0:T(8,128)S(1)}, s32[]{:T(128)}, bf16[4,2,4]{2,1,0:T(2,128)(2,1)}, ...), condition=%wide.region_5.6_spmd.clone, body=%wide.region_4.5_spmd.clone.sunk | while | flops 327692 | bytes 655545 | solution.py:54
  134.8 5.6 %fusion.20 = f32[4,128,2,4,64]{1,4,3,2,0:T(8,128)S(1)} fusion(f32[4,128,2,4,64]{1,0,4,3,2:T(4,128)} %reshape.174, f32[2,4,128,128]{3,2,0,1:T(8,128)} %fusion.72, f32[2,4,4,128]{3,1,0,2:T(4,128)S(1)} %bitcast.194, f32[2,4,4,128]{3,1,0,2:T(4,128)S(1)} %copy-done.21, pred[128,128]{1,0:T(8,128)(4,1)S(1)} %copy-done.19), kind=kOutput, calls=%fused_computation.37 | convolution fusion | flops 404750336 | bytes 2670592 | tf_op jit(solution)/shard_map/gkbij,bjgkp->bigkp/dot_general | solution.py:86
  157.1 9.8 %while.58 = (s32[]{:T(128)}, f32[2,4,64,128]{3,2,1,0:T(8,128)S(1)}, f32[4,2,4,64,128]{4,3,2,1,0:T(8,128)}, f32[4,2,4]{2,1,0:T(2,128)}, f32[4,2,4,64,128]{4,3,2,1,0:T(8,128)}, /*index=5*/s32[]{:T(128)}, s32[]{:T(128)}) while((s32[]{:T(128)}, f32[2,4,64,128]{3,2,1,0:T(8,128)S(1)}, f32[4,2,4,64,128]{4,3,2,1,0:T(8,128)}, ...), condition=%wide.region_9.10_spmd.clone, body=%wide.region_8.9_spmd.clone.sunk | while | flops 262147 | bytes 1311424 | solution.py:98
  166.9 10.7 %all-gather.3 = bf16[8,4,64,128]{3,2,1,0:T(8,128)(2,1)} all-gather(bf16[2,4,64,128]{3,2,1,0:T(8,128)(2,1)S(1)} %convert_element_type.232), channel_id=5, replica_groups=mesh['sp'=4,'tp'=8] {'sp'}, dimensions={0}, use_global_device_ids=true | all-gather | bytes 655360 | tf_op jit(solution)/shard_map/all_gather | solution.py:36
  177.6 6.8 %while.59 = (s32[]{:T(128)}, f32[2,4,64,128]{3,2,1,0:T(8,128)S(1)}, s32[]{:T(128)}, bf16[4,2,4]{2,1,0:T(2,128)(2,1)}, bf16[4,2,4,64,128]{4,3,2,1,0:T(8,128)(2,1)...) while((s32[]{:T(128)}, f32[2,4,64,128]{3,2,1,0:T(8,128)S(1)}, s32[]{:T(128)}, ...), condition=%wide.region_12.13_spmd.clone, body=%wide.region_11.12_spmd.clone.sunk | while | flops 327696 | bytes 655607 | solution.py:54
  184.4 5.6 %fusion.23 = f32[4,128,2,4,64]{1,4,3,2,0:T(8,128)S(1)} fusion(f32[4,128,2,4,64]{1,0,4,3,2:T(4,128)} %reshape.178, f32[2,4,128,128]{3,2,0,1:T(8,128)} %fusion.69, f32[2,4,4,128]{3,1,0,2:T(4,128)S(1)} %bitcast.193, f32[2,4,4,128]{3,1,0,2:T(4,128)S(1)} %copy-done.20, pred[128,128]{1,0:T(8,128)(4,1)S(1)} %copy-done.19), kind=kOutput, calls=%fused_computation.38 | convolution fusion | flops 404750336 | bytes 2670592 | tf_op jit(solution)/shard_map/gkbij,bjgkp->bigkp/dot_general | solution.py:86
  192.1 6.0 %rev.26 = f32[512,512]{0,1:T(8,128)} reverse(f32[512,512]{0,1:T(8,128)S(1)} %bitcast.183), dimensions={0} | reverse | bytes 2097152 | tf_op jit(solution)/shard_map/jit(_flip)/rev | solution.py:227
  204.2 35.4 %reduce-scatter.3.cloned.1.call-done = bf16[64,2048]{1,0:T(8,128)(2,1)} async-done(((bf16[512,2048]{1,0:T(8,128)(2,1)}), bf16[64,2048]{1,0:T(8,128)(2,1)}) %reduce-scatter.3.cloned.1.call-update) | async-done | bytes 262160 | tf_op jit(solution)/shard_map/reduce_scatter | solution.py:232
  242.6 12.0 %all_to_all.33 = bf16[24,8,2048]{2,0,1:T(8,128)(2,1)S(1)} all-to-all(bf16[24,8,2048]{2,0,1:T(8,128)(2,1)S(1)} %copy.213), channel_id=1, replica_groups=mesh['sp'=4,'tp'=8] {'sp'}, dimensions={1} | all-to-all | bytes 1572864 | tf_op jit(solution)/shard_map/all_to_all | solution.py:263
  255.9 63.8 %all-gather.8.cloned.1.call-done = bf16[768,2,2048]{2,0,1:T(8,128)(2,1)} async-done(((bf16[96,2,2048]{2,0,1:T(8,128)(2,1)}), bf16[768,2,2048]{2,0,1:T(8,128)(2,1)}) %all-gather.8.cloned.1.call-update) | async-done | bytes 6291472 | tf_op jit(solution)/shard_map/all_gather | solution.py:264
  319.7 9.1 %fusion.107 = f32[2,768,512]{2,1,0:T(8,128)} fusion(bf16[768,2,2048]{2,0,1:T(8,128)(2,1)} %all-gather.8.cloned.1.call-done, bf16[2,2048,512]{2,1,0:T(8,128)(2,1)} %param.42), kind=kOutput, calls=%fused_computation.197 | convolution fusion | flops 3221225472 | bytes 13631488 | tf_op jit(solution)/shard_map/red,edf->ref/dot_general | solution.py:268
  328.7 12.5 %convert_bitcast_fusion = bf16[768,2,2048]{2,0,1:T(8,128)(2,1)} fusion(bf16[2,512,2048]{2,1,0:T(8,128)(2,1)} %param.43, f32[2,768,512]{2,1,0:T(8,128)} %fusion.107, bf16[768,2,2048]{2,0,1:T(8,128)(2,1)} %all-gather.8.cloned.1.call-done, bf16[2,2048,512]{2,1,0:T(8,128)(2,1)} %param.41), kind=kOutput, calls=%fused_computation.12 | convolution fusion | flops 6450315264 | bytes 24117248 | tf_op jit(solution)/shard_map/ref,efd->red/dot_general | solution.py:273
  341.2 68.5 %reduce-scatter.5.cloned.1.call-done = bf16[96,2,2048]{2,0,1:T(8,128)(2,1)} async-done(((bf16[768,2,2048]{2,0,1:T(8,128)(2,1)}), bf16[96,2,2048]{2,0,1:T(8,128)(2,1)}) %reduce-scatter.5.cloned.1.call-update) | async-done | bytes 786448 | tf_op jit(solution)/shard_map/reduce_scatter | solution.py:272
  412.6 3.8 all-to-all-start.1
  416.4 9.1 %all-to-all-done.1 = bf16[96,2,2048]{2,1,0:T(2,128)(2,1)S(1)} async-done(((bf16[96,2,2048]{2,1,0:T(2,128)(2,1)}), bf16[96,2,2048]{2,1,0:T(2,128)(2,1)S(1)}, u32[]{:S(2)}, u32[]{:S(2)}) %all-to-all-start.1) | async-done | bytes 786464 | tf_op jit(solution)/shard_map/all_to_all | solution.py:280
  (211 shorter events, 124.0 us)
Async XLA Ops:
  6.5 193.9 %copy-start = (bf16[512,2048]{1,0:T(8,128)(2,1)S(1)}, bf16[512,2048]{1,0:T(8,128)(2,1)}, u32[]{:S(2)}) copy-start(bf16[512,2048]{1,0:T(8,128)(2,1)} %param.39) | copy-start | bytes 6291460
  6.5 56.1 %copy-start.9 = (bf16[512,256]{1,0:T(8,128)(2,1)S(1)}, bf16[512,256]{1,0:T(8,128)(2,1)}, u32[]{:S(2)}) copy-start(bf16[512,256]{1,0:T(8,128)(2,1)} %param.31) | copy-start | bytes 786436
  6.5 233.0 %reduce-scatter.3.cloned.1.call-start = ((), (), s32[]{:S(2)}) async-start(), calls=%async_computation.4 | async-start | bytes 2359296 | tf_op jit(solution)/shard_map/reduce_scatter | solution.py:232
  9.1 49.0 %collective-permute-start = (bf16[2,1024]{0,1:T(8,128)(2,1)}, bf16[2,1024]{0,1:T(8,128)(2,1)}, u32[]{:S(2)}, u32[]{:S(2)}) collective-permute-start(bf16[2,1024]{0,1:T(8,128)(2,1)} %copy.175), channel_id=1, source_target_pairs={{0,8},{8,16},{16,24},{1,9},{9,17},{17,25},{2,10},{10,18},{18,26},{... | collective-permute-start | bytes 12296 | tf_op jit(solution)/shard_map/ppermute | solution.py:25
  15.5 44.0 %collective-permute-start.1 = (bf16[2,1024]{0,1:T(8,128)(2,1)}, bf16[2,1024]{0,1:T(8,128)(2,1)}, u32[]{:S(2)}, u32[]{:S(2)}) collective-permute-start(bf16[2,1024]{0,1:T(8,128)(2,1)} %copy.178), channel_id=1, source_target_pairs={{8,0},{16,8},{24,16},{9,1},{17,9},{25,17},{10,2},{18,10},{26,18},{... | collective-permute-start | bytes 12296 | tf_op jit(solution)/shard_map/ppermute | solution.py:28
  64.5 18.8 %copy-start.23 = (f32[1,512]{1,0:T(1,128)S(1)}, f32[1,512]{1,0:T(1,128)}, u32[]{:S(2)}) copy-start(f32[1,512]{1,0:T(1,128)} %get-tuple-element.481) | copy-start | bytes 6148
  64.5 18.9 %copy-start.24 = (f32[1,512]{1,0:T(1,128)S(1)}, f32[1,512]{1,0:T(1,128)}, u32[]{:S(2)}) copy-start(f32[1,512]{1,0:T(1,128)} %get-tuple-element.482) | copy-start | bytes 6148
  64.6 18.9 %copy-start.25 = (f32[1,512]{1,0:T(1,128)S(1)}, f32[1,512]{1,0:T(1,128)}, u32[]{:S(2)}) copy-start(f32[1,512]{1,0:T(1,128)} %get-tuple-element.483) | copy-start | bytes 6148
  64.6 18.9 %copy-start.26 = (f32[1,512]{1,0:T(1,128)S(1)}, f32[1,512]{1,0:T(1,128)}, u32[]{:S(2)}) copy-start(f32[1,512]{1,0:T(1,128)} %get-tuple-element.484) | copy-start | bytes 6148
  64.6 18.9 %copy-start.27 = (f32[1,512]{1,0:T(1,128)S(1)}, f32[1,512]{1,0:T(1,128)}, u32[]{:S(2)}) copy-start(f32[1,512]{1,0:T(1,128)} %get-tuple-element.485) | copy-start | bytes 6148
  88.1 15.3 %copy-start.10 = (f32[4,128,2,4]{1,0,3,2:T(4,128)S(1)}, f32[4,128,2,4]{1,0,3,2:T(4,128)}, u32[]{:S(2)}) copy-start(f32[4,128,2,4]{1,0,3,2:T(4,128)} %get-tuple-element.476) | copy-start | bytes 49156
  117.8 17.0 %copy-start.16 = (f32[1,8,512]{2,1,0:T(8,128)S(1)}, f32[1,8,512]{2,1,0:T(8,128)}, u32[]{:S(2)}) copy-start(f32[1,8,512]{2,1,0:T(8,128)} %copy-done.15) | copy-start | bytes 49156
  117.8 17.0 %copy-start.19 = (pred[128,128]{1,0:T(8,128)(4,1)S(1)}, pred[128,128]{1,0:T(8,128)(4,1)}, u32[]{:S(2)}) copy-start(pred[128,128]{1,0:T(8,128)(4,1)} %iota_compare_fusion.3) | copy-start | bytes 49156
  117.8 17.0 %copy-start.21 = (f32[2,4,4,128]{3,1,0,2:T(4,128)S(1)}, f32[2,4,4,128]{3,1,0,2:T(4,128)}, u32[]{:S(2)}) copy-start(f32[2,4,4,128]{3,1,0,2:T(4,128)} %copy.180) | copy-start | bytes 49156
  166.9 17.5 %copy-start.14 = (f32[8,512]{1,0:T(8,128)S(1)}, f32[8,512]{1,0:T(8,128)}, u32[]{:S(2)}) copy-start(f32[8,512]{1,0:T(8,128)} %copy-done.13) | copy-start | bytes 49156
  166.9 17.5 %copy-start.20 = (f32[2,4,4,128]{3,1,0,2:T(4,128)S(1)}, f32[2,4,4,128]{3,1,0,2:T(4,128)}, u32[]{:S(2)}) copy-start(f32[2,4,4,128]{3,1,0,2:T(4,128)} %copy.197) | copy-start | bytes 49156
  200.5 39.1 %copy-start.7 = (bf16[64,2048]{1,0:T(8,128)(2,1)S(1)}, bf16[64,2048]{1,0:T(8,128)(2,1)}, u32[]{:S(2)}) copy-start(bf16[64,2048]{1,0:T(8,128)(2,1)} %param.27) | copy-start | bytes 786436
  200.5 40.3 %copy-start.22 = (f32[2048]{0:T(1024)S(1)}, f32[2048]{0:T(1024)}, u32[]{:S(2)}) copy-start(f32[2048]{0:T(1024)} %param.40) | copy-start | bytes 24580
  203.1 116.5 %all-gather.8.cloned.1.call-start = ((), (), s32[]{:S(2)}) async-start(), calls=%async_computation.5 | async-start | bytes 7077888 | tf_op jit(solution)/shard_map/all_gather | solution.py:264
  255.6 154.2 %reduce-scatter.5.cloned.1.call-start = ((), (), s32[]{:S(2)}) async-start(), calls=%async_computation.6 | async-start | bytes 7077888 | tf_op jit(solution)/shard_map/reduce_scatter | solution.py:272
  341.2 75.2 %copy-start.29 = (f32[64,2]{0,1:T(2,128)S(1)}, f32[64,2]{0,1:T(2,128)}, u32[]{:S(2)}) copy-start(f32[64,2]{0,1:T(2,128)} %param.45) | copy-start | bytes 1540
  412.6 17.2 %copy-start.8 = (bf16[64,2048]{1,0:T(8,128)(2,1)S(1)}, bf16[64,2048]{1,0:T(8,128)(2,1)}, u32[]{:S(2)}) copy-start(bf16[64,2048]{1,0:T(8,128)(2,1)} %reduce-scatter.3.cloned.1.call-done) | copy-start | bytes 786436
  412.6 12.9 %all-to-all-start.1 = ((bf16[96,2,2048]{2,1,0:T(2,128)(2,1)}), bf16[96,2,2048]{2,1,0:T(2,128)(2,1)S(1)}, u32[]{:S(2)}, u32[]{:S(2)}) async-start(bf16[96,2,2048]{2,1,0:T(2,128)(2,1)} %copy.215), calls=%async_computation.3 | async-start | bytes 1572864 | tf_op jit(solution)/shard_map/all_to_all | solution.py:280
  416.4 14.2 %copy-start.1 = (bf16[512,2048]{1,0:T(8,128)(2,1)S(1)}, bf16[512,2048]{1,0:T(8,128)(2,1)}, u32[]{:S(2)}) copy-start(bf16[512,2048]{1,0:T(8,128)(2,1)} %param.39) | copy-start | bytes 6291460
  (13 other events, 100.3 us)
Sparse Core Ops, SparseCore 0:
  203.2 36.2 reduce-scatter.2
  255.7 63.9 all-gather.7
  341.3 68.3 reduce-scatter.4
where the time goes:
time: 441 us; the launch traced here: 437 us
  waiting for transfers between devices  177 us (40%)
  local copies, waits for them, and re-layouts  76.9 us (17%)
  other arithmetic  57.6 us (13%)
  blocking collectives  50.7 us (11%)
  matrix products  50.2 us (11%)
  between operations  13.7 us (3%)
  starting transfers between devices  11 us (2%)
    reduce_scatter x1, waiting for transfers between devices, per_device(): lax.psum_scatter(jnp.einsum('ref,efd->red', hidden, specialist_contract_m...  68.5 us
    all_gather x1, waiting for transfers between devices, per_device(): data_block = lax.all_gather(received, 'tp', axis=0, tiled=True)  63.8 us
    all_gather x4, blocking collectives, prefix(): lax.all_gather(part.astype(kind), axis)  38.7 us
    reduce_scatter x1, waiting for transfers between devices, per_device(): lax.psum_scatter(jnp.dot(mixed_rows, blend_result_matrix, preferred_eleme...  35.4 us
    dot_general x1, matrix products, per_device(): jnp.einsum('ref,efd->red', hidden, specialist_contract_matrix, preferred_...  12.5 us
    all_to_all x1, blocking collectives, per_device(): lax.all_to_all(buffer, 'sp', split_axis=1, concat_axis=0, tiled=True)  12 us
    dot_general x2, matrix products, local_sweep(): jnp.einsum('gkbij,bjgkp->bigkp', mixing, values, precision=HIGHEST_MODE)  11.3 us
    mul x3, other arithmetic, centred_conv(): return jax.nn.silu(summed)  9.7 us
  transfers between devices with their start and end apart: 6, of which 4 were waited for; matrix products, arithmetic and copies ran while one was open for 6% of the time, Pallas kernels for 0%

commit v1 on v0

v1 whole, which is shorter than its diff:
```python
import functools
import math

import jax
import jax.numpy as jnp
from jax import lax
from jax.experimental import pallas as pl
from jax.experimental.pallas import tpu as pltpu
from jax.sharding import PartitionSpec as P

HEAD_DIM = 64
STATE = 128
TOP = 2
TILE = 128
PAD = 8
EXTRA = 16

EPSILON = 1e-06
LOG2E = math.log2(math.e)
F32, BF16 = jnp.float32, jnp.bfloat16


def silu(v):
    return v / (1.0 + jnp.exp(-v))


def over_heads(columns, first, count):
    rows = columns.shape[0]
    lane = lax.broadcasted_iota(jnp.int32, (rows, 2 * HEAD_DIM), 1)
    pairs = []
    for h in range(0, count, 2):
        a = jnp.broadcast_to(columns[:, first + h : first + h + 1], lane.shape)
        b = jnp.broadcast_to(columns[:, first + h + 1 : first + h + 2], lane.shape)
        pairs.append(jnp.where(lane < HEAD_DIM, a, b))
    return jnp.concatenate(pairs, axis=1)


def prepare_kernel(
    x_ref, b_ref, c_ref, low_ref, high_ref, tx_ref, tb_ref, tc_ref, raw_ref, speed_ref, fade_ref,
    xc_ref, bc_ref, cc_ref, rows_ref, cols_ref, *rest, axis,
):
    *msg_refs, pad_ref = rest
    steps = x_ref.shape[0]
    heads = raw_ref.shape[1]
    groups = b_ref.shape[1] // STATE
    per_group = heads // groups
    wide = per_group * HEAD_DIM
    here = lax.axis_index(axis)

    lane = lax.broadcasted_iota(jnp.int32, (heads, steps), 1)
    eye = lax.broadcasted_iota(jnp.int32, (heads, heads), 0) == lax.broadcasted_iota(
        jnp.int32, (heads, heads), 1
    )
    sums, weights, totals = [], [], []
    for d in range(2):
        raw = raw_ref[d].astype(F32)
        step = jnp.maximum(raw, 0.0) + jnp.log1p(jnp.exp(-jnp.abs(raw)))
        speed = jnp.sum(
            jnp.where(eye, jnp.exp(speed_ref[d : d + 1, :]), 0.0), axis=1, keepdims=True
        )
        run = -step * speed + fade_ref[d]
        shift = 1
        while shift < steps:
            if d == 0:
                run = run + jnp.where(lane >= shift, pltpu.roll(run, shift, 1), 0.0)
            else:
                run = run + jnp.where(lane < steps - shift, pltpu.roll(run, steps - shift, 1), 0.0)
            shift *= 2
        total = run[:, steps - 1 : steps] if d == 0 else run[:, 0:1]
        totals.append(total)
        sums.append(run * LOG2E)
        weights.append(jnp.exp(total - run) * step)
        rows_ref[d] = run * LOG2E - jnp.log(step) * LOG2E
    stacked = jnp.concatenate(
        sums + weights + [jnp.zeros((STATE - 4 * heads, steps), F32)], axis=0
    )
    cols = stacked.T
    cols_ref[...] = cols

    def conv(ref, taps_ref, at, start):
        pad_ref[PAD - 2 : PAD] = low_ref[:, at + start : at + start + TILE].astype(F32)
        pad_ref[PAD : PAD + steps] = ref[:, start : start + TILE].astype(F32)
        pad_ref[PAD + steps : PAD + steps + 2] = high_ref[
            :, at + start : at + start + TILE
        ].astype(F32)
        taps = taps_ref[:, start : start + TILE].astype(F32)
        total = taps[0:1] * pad_ref[PAD - 2 : PAD - 2 + steps]
        for j in range(1, taps.shape[0]):
            total = total + taps[j : j + 1] * pad_ref[PAD - 2 + j : PAD - 2 + j + steps]
        return silu(total)

    at = 0
    for ref, taps_ref, out_ref in (
        (x_ref, tx_ref, xc_ref), (b_ref, tb_ref, bc_ref), (c_ref, tc_ref, cc_ref),
    ):
        for start in range(0, ref.shape[1], TILE):
            out_ref[:, start : start + TILE] = conv(ref, taps_ref, at, start).astype(BF16)
        at += ref.shape[1]

    row = lax.broadcasted_iota(jnp.int32, (EXTRA, wide), 0)
    own = lax.broadcasted_iota(jnp.int32, (per_group, wide), 0) == (
        lax.broadcasted_iota(jnp.int32, (per_group, wide), 1) // HEAD_DIM
    )
    for g in range(groups):
        turned = bc_ref[:, g * STATE : (g + 1) * STATE].astype(F32).T.astype(BF16)
        xg = xc_ref[:, g * wide : (g + 1) * wide].astype(F32)
        both = []
        for d in range(2):
            weight = over_heads(cols, (2 + d) * heads + g * per_group, per_group)
            state = jnp.dot(turned, (xg * weight).astype(BF16), preferred_element_type=F32)
            total = jnp.sum(
                jnp.where(own, totals[d][g * per_group : (g + 1) * per_group], 0.0),
                axis=0, keepdims=True,
            )
            upper = total.astype(BF16).astype(F32)
            extra = jnp.where(row == 0, upper, jnp.where(row == 1, total - upper, 0.0))
            both.append((state, extra))
        for k, msg_ref in enumerate(msg_refs, 1):
            onward = jnp.where((here ^ k) > here, 1.0, 0.0).astype(F32)
            (sf, ef), (sb, eb) = both
            msg_ref[g, 0:STATE, :] = (sf * onward + sb * (1.0 - onward)).astype(BF16)
            msg_ref[g, STATE : STATE + EXTRA, :] = (ef * onward + eb * (1.0 - onward)).astype(BF16)


def local_kernel(xc_ref, bc_ref, cc_ref, rows_ref, cols_ref, y_ref):
    steps = xc_ref.shape[0]
    heads = rows_ref.shape[1]
    groups = bc_ref.shape[1] // STATE
    per_group = heads // groups
    tiles = steps // TILE
    i_at = lax.broadcasted_iota(jnp.int32, (TILE, TILE), 0)
    j_at = lax.broadcasted_iota(jnp.int32, (TILE, TILE), 1)
    for g in range(groups):
        for i in range(tiles):
            span = slice(i * TILE, (i + 1) * TILE)
            inner = lax.dot_general(
                cc_ref[span, g * STATE : (g + 1) * STATE],
                bc_ref[:, g * STATE : (g + 1) * STATE],
                (((1,), (1,)), ((), ())),
                preferred_element_type=F32,
            )
            for pair in range(per_group // 2):
                halves = []
                at = (g * per_group + 2 * pair) * HEAD_DIM
                for h in (g * per_group + 2 * pair, g * per_group + 2 * pair + 1):
                    here_f = jnp.broadcast_to(cols_ref[span, h : h + 1], (TILE, TILE))
                    here_b = jnp.broadcast_to(cols_ref[span, heads + h : heads + h + 1], (TILE, TILE))
                    parts = []
                    for j in range(tiles):
                        js = slice(j * TILE, (j + 1) * TILE)
                        if j <= i:
                            mix = jnp.exp2(here_f - rows_ref[0, h : h + 1, js])
                            if j == i:
                                mix = jnp.where(i_at >= j_at, mix, 0.0) + jnp.where(
                                    i_at <= j_at, jnp.exp2(here_b - rows_ref[1, h : h + 1, js]), 0.0
                                )
                        else:
                            mix = jnp.exp2(here_b - rows_ref[1, h : h + 1, js])
                        parts.append((mix * inner[:, js]).astype(BF16))
                    halves.append(
                        jnp.dot(
                            jnp.concatenate(parts, axis=1),
                            xc_ref[:, at : at + 2 * HEAD_DIM],
                            preferred_element_type=F32,
                        )
                    )
                y_ref[span, at : at + 2 * HEAD_DIM] = jnp.where(j_at < HEAD_DIM, *halves)


def finish_kernel(y_ref, cc_ref, cols_ref, switch_ref, gain_ref, *rest, axis):
    *msg_refs, out_ref, carry_ref = rest
    steps, channels = y_ref.shape
    groups = cc_ref.shape[1] // STATE
    wide = channels // groups
    per_group = wide // HEAD_DIM
    heads = groups * per_group
    here = lax.axis_index(axis)
    peers = [here ^ k for k in range(1, len(msg_refs) + 1)]

    def flag(condition):
        return jnp.where(condition, 1.0, 0.0).astype(F32)

    for g in range(groups):
        totals = [
            ref[g, STATE : STATE + 1, :].astype(F32) + ref[g, STATE + 1 : STATE + 2, :].astype(F32)
            for ref in msg_refs
        ]
        for d in range(2):
            carry = jnp.zeros((STATE, wide), F32)
            for k, ref in enumerate(msg_refs):
                between = jnp.zeros((1, wide), F32)
                for other in range(len(msg_refs)):
                    if other != k:
                        if d == 0:
                            inside = (peers[k] < peers[other]) & (peers[other] < here)
                        else:
                            inside = (peers[k] > peers[other]) & (peers[other] > here)
                        between = between + flag(inside) * totals[other]
                mine = flag(peers[k] < here if d == 0 else peers[k] > here)
                carry = carry + ref[g, 0:STATE, :].astype(F32) * (mine * jnp.exp(between))
            carry_ref[d] = carry.astype(BF16)
        for i in range(steps // TILE):
            span = slice(i * TILE, (i + 1) * TILE)
            lanes = slice(g * wide, (g + 1) * wide)
            cols = jnp.exp2(cols_ref[span, :])
            cc = cc_ref[span, g * STATE : (g + 1) * STATE]
            y = y_ref[span, lanes]
            for d in range(2):
                y = y + over_heads(cols, d * heads + g * per_group, per_group) * jnp.dot(
                    cc, carry_ref[d], preferred_element_type=F32
                )
            gated = y * silu(switch_ref[span, lanes].astype(F32))
            mean = jnp.sum(gated * gated, axis=1, keepdims=True) * (1.0 / wide)
            out_ref[span, lanes] = (
                gated * lax.rsqrt(mean + EPSILON) * gain_ref[:, lanes]
            ).astype(BF16)


def vmem(count):
    return [pl.BlockSpec(memory_space=pltpu.VMEM) for _ in range(count)]


def mixer(x, b, c, tx, tb, tc, raw, speed, fade, switch, gain):
    steps, channels = x.shape
    heads = raw.shape[1]
    groups = b.shape[1] // STATE
    wide = channels // groups
    rim = tx.shape[0] // 2
    count = lax.axis_size("sp")
    first = jnp.concatenate([x[:rim], b[:rim], c[:rim]], axis=1)
    last = jnp.concatenate([x[-rim:], b[-rim:], c[-rim:]], axis=1)
    low = lax.ppermute(last, "sp", [(i, i + 1) for i in range(count - 1)])
    high = lax.ppermute(first, "sp", [(i + 1, i) for i in range(count - 1)])
    message = jax.ShapeDtypeStruct((groups, STATE + EXTRA, wide), BF16)
    xc, bc, cc, rows, cols, *sends = pl.pallas_call(
        functools.partial(prepare_kernel, axis="sp"),
        out_shape=[
            jax.ShapeDtypeStruct(x.shape, BF16),
            jax.ShapeDtypeStruct(b.shape, BF16),
            jax.ShapeDtypeStruct(c.shape, BF16),
            jax.ShapeDtypeStruct((2, heads, steps), F32),
            jax.ShapeDtypeStruct((steps, STATE), F32),
        ]
        + [message] * (count - 1),
        in_specs=vmem(11),
        out_specs=vmem(5 + count - 1),
        scratch_shapes=[pltpu.VMEM((steps + 2 * PAD, TILE), F32)],
        name="prepare",
    )(x, b, c, low, high, tx, tb, tc, raw, speed, fade)
    arrived = [
        lax.ppermute(send, "sp", [(i, i ^ k) for i in range(count)])
        for k, send in enumerate(sends, 1)
    ]
    y = pl.pallas_call(
        local_kernel,
        out_shape=jax.ShapeDtypeStruct(x.shape, F32),
        in_specs=vmem(5),
        out_specs=vmem(1)[0],
        cost_estimate=pl.CostEstimate(
            flops=2 * steps * steps * (channels + groups * STATE) * 4,
            bytes_accessed=8 * steps * channels,
            transcendentals=heads * steps * steps,
        ),
        name="local",
    )(xc, bc, cc, rows, cols)
    return pl.pallas_call(
        functools.partial(finish_kernel, axis="sp"),
        out_shape=jax.ShapeDtypeStruct(x.shape, BF16),
        in_specs=vmem(5 + count - 1),
        out_specs=vmem(1)[0],
        scratch_shapes=[pltpu.VMEM((2, STATE, wide), BF16)],
        name="finish",
    )(y, cc, cols, switch, gain.reshape(1, -1), *arrived)


def rms_scale(stream, gain):
    values = stream.astype(jnp.float32)
    return (
        values * lax.rsqrt(jnp.mean(values * values, axis=-1, keepdims=True) + EPSILON) * gain
    ).astype(jnp.bfloat16)


def per_device(
    skip_stream_entry,
    result_switch_mapped,
    channel_feed_mapped,
    write_coefficient_mapped,
    emission_coefficient_mapped,
    channel_feed_taps,
    write_coefficient_taps,
    emission_coefficient_taps,
    raw_increments,
    channel_log_fade_speed,
    extra_log_fade,
    cluster_scaling_factor,
    blend_result_matrix,
    routing_scaling_factor,
    specialist_switch_matrix,
    specialist_widen_matrix,
    specialist_contract_matrix,
    picked_specialists,
    router_affinities,
):
    mixed_rows = mixer(
        channel_feed_mapped,
        write_coefficient_mapped,
        emission_coefficient_mapped,
        channel_feed_taps,
        write_coefficient_taps,
        emission_coefficient_taps,
        raw_increments,
        channel_log_fade_speed,
        extra_log_fade,
        result_switch_mapped,
        cluster_scaling_factor,
    )
    rows_here = skip_stream_entry.shape[0]
    projected = lax.psum_scatter(
        jnp.dot(mixed_rows, blend_result_matrix, preferred_element_type=jnp.float32).astype(
            jnp.bfloat16
        ),
        "tp",
        scatter_dimension=0,
        tiled=True,
    ).astype(jnp.float32)
    after_mixer = (skip_stream_entry.astype(jnp.float32) + projected).astype(jnp.bfloat16)
    normed = rms_scale(after_mixer, routing_scaling_factor)
    experts_here = specialist_switch_matrix.shape[0]
    expert_count = experts_here * lax.axis_size("sp")
    capacity = max(2, 3 * TOP * rows_here // (2 * expert_count))
    slot_total = capacity * expert_count
    flat_routes = picked_specialists.reshape(-1)
    one_hot = (flat_routes[:, None] == jnp.arange(expert_count, dtype=jnp.int32)[None, :]).astype(
        jnp.int32
    )
    earlier_count = jnp.cumsum(one_hot, axis=0) - one_hot
    slot_rank = jnp.sum(earlier_count * one_hot, axis=1)
    position = slot_rank * expert_count + flat_routes
    slot_match = (position[:, None] == jnp.arange(slot_total, dtype=jnp.int32)[None, :]).astype(
        jnp.bfloat16
    )
    buffer = jnp.einsum(
        "rks,rd->sd",
        slot_match.reshape(rows_here, TOP, slot_total),
        normed,
        preferred_element_type=jnp.float32,
    ).astype(jnp.bfloat16)
    buffer = buffer.reshape(capacity, expert_count, skip_stream_entry.shape[1])
    received = lax.all_to_all(buffer, "sp", split_axis=1, concat_axis=0, tiled=True)
    data_block = lax.all_gather(received, "tp", axis=0, tiled=True)
    gate_part = jnp.einsum(
        "red,edf->ref", data_block, specialist_switch_matrix, preferred_element_type=jnp.float32
    )
    up_part = jnp.einsum(
        "red,edf->ref", data_block, specialist_widen_matrix, preferred_element_type=jnp.float32
    )
    hidden = (jax.nn.silu(gate_part) * up_part).astype(jnp.bfloat16)
    expert_out = lax.psum_scatter(
        jnp.einsum(
            "ref,efd->red", hidden, specialist_contract_matrix, preferred_element_type=jnp.float32
        ).astype(jnp.bfloat16),
        "tp",
        scatter_dimension=0,
        tiled=True,
    )
    returned = lax.all_to_all(expert_out, "sp", split_axis=0, concat_axis=1, tiled=True)
    picked = jnp.dot(
        slot_match, returned.reshape(slot_total, skip_stream_entry.shape[1]), preferred_element_type=jnp.float32
    )
    weights = router_affinities / jnp.sum(router_affinities, axis=-1, keepdims=True)
    mixture = jnp.sum(weights[..., None] * picked.reshape(rows_here, TOP, skip_stream_entry.shape[1]), axis=1)
    return (after_mixer.astype(jnp.float32) + mixture).astype(jnp.bfloat16)


def solution(mesh):
    in_specs = (
        P(("sp", "tp"), None),
        P("sp", "tp"),
        P("sp", "tp"),
        P("sp", "tp"),
        P("sp", "tp"),
        P(None, "tp"),
        P(None, "tp"),
        P(None, "tp"),
        P(None, "tp", "sp"),
        P(None, "tp"),
        P(None, "tp", "sp"),
        P("tp"),
        P("tp", None),
        P(),
        P("sp", None, "tp"),
        P("sp", None, "tp"),
        P("sp", "tp", None),
        P(("sp", "tp"), None),
        P(("sp", "tp"), None),
    )
    out_specs = P(("sp", "tp"), None)
    return jax.shard_map(
        per_device, mesh=mesh, in_specs=in_specs, out_specs=out_specs, check_vma=False
    )
```

time: 441 us -> 278 us (0.63)
  local copies, waits for them, and re-layouts: 76.9 us -> 11.6 us
  other arithmetic: 57.6 us -> 2.52 us
  blocking collectives: 50.7 us -> 12 us
  matrix products: 50.2 us -> 26.9 us
  Pallas kernels: 0 us -> 15.3 us
  waiting for transfers between devices: 177 us -> 182 us
    all_gather x4 -> x0, blocking collectives: 38.7 us -> none  [prefix(): lax.all_gather(part.astype(kind), axis)]
    rev x6 -> x0, local copies, waits for them, and re-layouts: 25.5 us -> none  [the longest x1 9.4 us: blend_parts_list(): jnp.flip(inputs, 0)]
    dot_general x9 -> x1, matrix products: 24.7 us -> 0.35 us  [per_device(): jnp.dot(slot_match, returned.reshape(slot_total, skip_stream_entry.shape[...]
    pallas_call x0 -> x3, Pallas kernels: none -> 15.3 us  [the longest x1 5.61 us: mixer(): pl.pallas_call(functools.partial(prepare_kernel, axis='sp'), out_shape=[j...]
    mul x6 -> x0, other arithmetic: 14.2 us -> none  [the longest x3 9.7 us: centred_conv(): return jax.nn.silu(summed)]
    reshape x9 -> x2, local copies, waits for them, and re-layouts: 15.5 us -> 2.7 us  [the longest x1 2.26 us: per_device(): returned.reshape(slot_total, skip_stream_entry.shape[1])]
    add x9 -> x0, other arithmetic: 9.2 us -> none  [the longest x8 8.36 us: advance(): carried * jnp.exp(decay_piece)[..., None, None] + state_piece]
    exp x13 -> x0, local copies, waits for them, and re-layouts: 8.46 us -> none  [the longest x8 5.2 us: advance(): jnp.exp(decay_piece)[..., None, None]]
  transfers between devices with their start and end apart: 6 -> 9, of which waited for: 4 -> 6; matrix products, arithmetic and copies ran while one was open for 6% -> 0% of each run, Pallas kernels for 0% -> 2%
where the time goes in v1:
time: 278 us; the launch traced here: 277 us
  waiting for transfers between devices  182 us (65%)
  matrix products  26.9 us (10%)
  Pallas kernels  15.3 us (6%)
  starting transfers between devices  14.1 us (5%)
  between operations  13.3 us (5%)
  blocking collectives  12 us (4%)
  local copies, waits for them, and re-layouts  11.6 us (4%)
    reduce_scatter x1, waiting for transfers between devices, per_device(): lax.psum_scatter(jnp.einsum('ref,efd->red', hidden, specialist_contract_m...  68.5 us
    all_gather x1, waiting for transfers between devices, per_device(): data_block = lax.all_gather(received, 'tp', axis=0, tiled=True)  63.9 us
    reduce_scatter x1, waiting for transfers between devices, per_device(): lax.psum_scatter(jnp.dot(mixed_rows, blend_result_matrix, preferred_eleme...  35.2 us
    dot_general x1, matrix products, per_device(): jnp.einsum('ref,efd->red', hidden, specialist_contract_matrix, preferred_...  12.5 us
    all_to_all x1, blocking collectives, per_device(): lax.all_to_all(buffer, 'sp', split_axis=1, concat_axis=0, tiled=True)  12 us
    all_to_all x1, waiting for transfers between devices, per_device(): lax.all_to_all(expert_out, 'sp', split_axis=0, concat_axis=1, tiled=True)  9.06 us
    dot_general x1, matrix products, per_device(): jnp.einsum('red,edf->ref', data_block, specialist_widen_matrix, preferred...  9.06 us
    pallas_call x1, Pallas kernels, mixer(): pl.pallas_call(functools.partial(prepare_kernel, axis='sp'), out_shape=[j...  5.61 us
  transfers between devices with their start and end apart: 9, of which 6 were waited for; matrix products, arithmetic and copies ran while one was open for 0% of the time, Pallas kernels for 2%

profile of v1, /device:TPU:0, one launch (start us, length us, event | category | flops | bytes accessed | tf_op | source)
XLA Modules:
  0.0 277.3 jit_solution(1717720969759524489)
XLA Ops:
  6.5 0.9 fusion.20
  8.2 4.9 %collective-permute-start = (bf16[2,1024]{1,0:T(2,128)(2,1)S(1)}, bf16[2,1024]{1,0:T(2,128)(2,1)S(1)}, u32[]{:S(2)}, u32[]{:S(2)}) collective-permute-start(bf16[2,1024]{1,0:T(2,128)(2,1)S(1)} %pad_maximum_fusion), channel_id=1, source_target_pairs={{0,8},{8,16},{16,24},{1,9},{9,17},{17,25},{2,10},{10,18},{18,26},{... | collective-permute-start | bytes 12296 | tf_op jit(solution)/shard_map/ppermute | solution.py:232
  13.1 1.3 collective-permute-start.1
  14.4 4.2 %collective-permute-done.1.high_ref = bf16[2,1024]{1,0:T(2,128)(2,1)S(1)} collective-permute-done((bf16[2,1024]{1,0:T(2,128)(2,1)S(1)}, bf16[2,1024]{1,0:T(2,128)(2,1)S(1)}, u32[]{:S(2)}, u32[]{:S(2)}) %collective-permute-start.1) | collective-permute-done | bytes 4128 | tf_op jit(solution)/shard_map/ppermute | solution.py:233
  19.1 5.6 %prepare.1 = (bf16[512,512]{1,0:T(8,128)(2,1)}, bf16[512,256]{1,0:T(8,128)(2,1)}, bf16[512,256]{1,0:T(8,128)(2,1)}, f32[2,8,512]{2,1,0:T(8,128)}, f32[512,128]{1...) custom-call(bf16[512,512]{1,0:T(8,128)(2,1)} %x_ref.1, ...), custom_call_target="tpu_custom_call" | custom-call | tf_op jit(solution)/shard_map/prepare/pallas_call | solution.py:235
  24.8 2.5 collective-permute-start.2
  27.2 1.5 collective-permute-start.4
  28.8 5.1 %local.1.y_ref = f32[512,512]{1,0:T(8,128)} custom-call(bf16[512,512]{1,0:T(8,128)(2,1)} %get-tuple-element.13.xc_ref, bf16[512,256]{1,0:T(8,128)(2,1)} %get-tuple-element.14.bc_ref, bf16[512,256]{1,0:T(8,128)(2,1)} %get-tuple-element.15.cc_ref, f32[2,8,512]{2,1,0:T(8,128)} %get-tuple-element.16.rows_ref, f32[512,128]{1,0:T(8,128)} %get-tuple-element.17.cols_ref), custom_call_target="tpu_custom_call" | custom-call | flops 1610612736 | bytes 2097152 | tf_op jit(solution)/shard_map/local/pallas_call | solution.py:254
  35.2 4.6 %finish.1 = bf16[512,512]{1,0:T(8,128)(2,1)} custom-call(f32[512,512]{1,0:T(8,128)} %local.1.y_ref, bf16[512,256]{1,0:T(8,128)(2,1)} %get-tuple-element.15.cc_ref, f32[512,128]{1,0:T(8,128)} %get-tuple-element.17.cols_ref, bf16[512,512]{1,0:T(8,128)(2,1)} %switch_ref.1, f32[1,512]{1,0:T(1,128)} %bitcast.50, bf16[2,144,256]{2,1,0:T(8,128)(2,1)} %copy-done.3, ...), custom_call_target="tpu_custom_call" | custom-call | tf_op jit(solution)/shard_map/finish/pallas_call | solution.py:266
  39.9 3.7 %convolution_convert_fusion = bf16[512,2048]{1,0:T(8,128)(2,1)} fusion(bf16[512,512]{1,0:T(8,128)(2,1)} %finish.1, bf16[512,2048]{1,0:T(8,128)(2,1)S(1)} %copy-done), kind=kOutput, calls=%fused_computation.8 | convolution fusion | flops 1074790400 | bytes 4718592 | tf_op jit(solution)/shard_map/dot_general | solution.py:319
  44.7 35.2 %reduce-scatter.3.cloned.1.call-done = bf16[64,2048]{1,0:T(8,128)(2,1)} async-done(((bf16[512,2048]{1,0:T(8,128)(2,1)}), bf16[64,2048]{1,0:T(8,128)(2,1)}) %reduce-scatter.3.cloned.1.call-update) | async-done | bytes 262160 | tf_op jit(solution)/shard_map/reduce_scatter | solution.py:318
  79.8 1.1 fusion.7
  81.0 1.4 fusion.4
  82.8 12.0 %all_to_all.33 = bf16[24,8,2048]{2,0,1:T(8,128)(2,1)S(1)} all-to-all(bf16[24,8,2048]{2,0,1:T(8,128)(2,1)S(1)} %copy.47), channel_id=1, replica_groups=mesh['sp'=4,'tp'=8] {'sp'}, dimensions={1} | all-to-all | bytes 1572864 | tf_op jit(solution)/shard_map/all_to_all | solution.py:349
  94.8 1.0 copy.48
  96.0 63.9 %all-gather.2.cloned.1.call-done = bf16[768,2,2048]{2,0,1:T(8,128)(2,1)} async-done(((bf16[96,2,2048]{2,0,1:T(8,128)(2,1)}), bf16[768,2,2048]{2,0,1:T(8,128)(2,1)}) %all-gather.2.cloned.1.call-update) | async-done | bytes 6291472 | tf_op jit(solution)/shard_map/all_gather | solution.py:350
  160.0 9.1 %fusion.23 = f32[2,768,512]{2,1,0:T(8,128)} fusion(bf16[768,2,2048]{2,0,1:T(8,128)(2,1)} %all-gather.2.cloned.1.call-done, bf16[2,2048,512]{2,1,0:T(8,128)(2,1)} %param.34), kind=kOutput, calls=%fused_computation.43 | convolution fusion | flops 3221225472 | bytes 13631488 | tf_op jit(solution)/shard_map/red,edf->ref/dot_general | solution.py:354
  169.0 12.5 %convert_bitcast_fusion = bf16[768,2,2048]{2,0,1:T(8,128)(2,1)} fusion(bf16[2,512,2048]{2,1,0:T(8,128)(2,1)} %param.35, f32[2,768,512]{2,1,0:T(8,128)} %fusion.23, bf16[768,2,2048]{2,0,1:T(8,128)(2,1)} %all-gather.2.cloned.1.call-done, bf16[2,2048,512]{2,1,0:T(8,128)(2,1)} %param.33), kind=kOutput, calls=%fused_computation | convolution fusion | flops 6450315264 | bytes 24117248 | tf_op jit(solution)/shard_map/ref,efd->red/dot_general | solution.py:359
  181.5 68.5 %reduce-scatter.5.cloned.1.call-done = bf16[96,2,2048]{2,0,1:T(8,128)(2,1)} async-done(((bf16[768,2,2048]{2,0,1:T(8,128)(2,1)}), bf16[96,2,2048]{2,0,1:T(8,128)(2,1)}) %reduce-scatter.5.cloned.1.call-update) | async-done | bytes 786448 | tf_op jit(solution)/shard_map/reduce_scatter | solution.py:358
  250.1 2.8 %copy.49 = bf16[96,2,2048]{2,1,0:T(2,128)(2,1)} copy(bf16[96,2,2048]{2,0,1:T(8,128)(2,1)} %reduce-scatter.5.cloned.1.call-done) | data formatting | bytes 1572864 | tf_op jit(solution)/shard_map/reduce_scatter | solution.py:358
  252.9 3.6 %all-to-all-start.1 = ((bf16[96,2,2048]{2,1,0:T(2,128)(2,1)}), bf16[96,2,2048]{2,1,0:T(2,128)(2,1)S(1)}, u32[]{:S(2)}, u32[]{:S(2)}) async-start(bf16[96,2,2048]{2,1,0:T(2,128)(2,1)} %copy.49), calls=%async_computation.3 | async-start | bytes 1572864 | tf_op jit(solution)/shard_map/all_to_all | solution.py:366
  256.5 9.1 %all-to-all-done.1 = bf16[96,2,2048]{2,1,0:T(2,128)(2,1)S(1)} async-done(((bf16[96,2,2048]{2,1,0:T(2,128)(2,1)}), bf16[96,2,2048]{2,1,0:T(2,128)(2,1)S(1)}, u32[]{:S(2)}, u32[]{:S(2)}) %all-to-all-start.1) | async-done | bytes 786464 | tf_op jit(solution)/shard_map/all_to_all | solution.py:366
  265.6 1.7 copy.52
  267.3 2.3 reshape.69
  (52 shorter events, 5.7 us)
Async XLA Ops:
  6.5 33.3 %copy-start = (bf16[512,2048]{1,0:T(8,128)(2,1)S(1)}, bf16[512,2048]{1,0:T(8,128)(2,1)}, u32[]{:S(2)}) copy-start(bf16[512,2048]{1,0:T(8,128)(2,1)} %param.31) | copy-start | bytes 6291460
  6.5 73.3 %reduce-scatter.3.cloned.1.call-start = ((), (), s32[]{:S(2)}) async-start(), calls=%async_computation.4 | async-start | bytes 2359296 | tf_op jit(solution)/shard_map/reduce_scatter | solution.py:318
  8.2 6.2 %collective-permute-start = (bf16[2,1024]{1,0:T(2,128)(2,1)S(1)}, bf16[2,1024]{1,0:T(2,128)(2,1)S(1)}, u32[]{:S(2)}, u32[]{:S(2)}) collective-permute-start(bf16[2,1024]{1,0:T(2,128)(2,1)S(1)} %pad_maximum_fusion), channel_id=1, source_target_pairs={{0,8},{8,16},{16,24},{1,9},{9,17},{17,25},{2,10},{10,18},{18,26},{... | collective-permute-start | bytes 12296 | tf_op jit(solution)/shard_map/ppermute | solution.py:232
  13.1 5.5 %collective-permute-start.1 = (bf16[2,1024]{1,0:T(2,128)(2,1)S(1)}, bf16[2,1024]{1,0:T(2,128)(2,1)S(1)}, u32[]{:S(2)}, u32[]{:S(2)}) collective-permute-start(bf16[2,1024]{1,0:T(2,128)(2,1)S(1)} %pad_maximum_fusion.1), channel_id=1, source_target_pairs={{8,0},{16,8},{24,16},{9,1},{17,9},{25,17},{10,2},{18,10},{26,18},{... | collective-permute-start | bytes 12296 | tf_op jit(solution)/shard_map/ppermute | solution.py:233
  14.4 4.2 %copy-start.7 = (bf16[2,1024]{1,0:T(2,128)(2,1)}, bf16[2,1024]{1,0:T(2,128)(2,1)S(1)}, u32[]{:S(2)}) copy-start(bf16[2,1024]{1,0:T(2,128)(2,1)S(1)} %collective-permute-done.low_ref) | copy-start | bytes 12292
  18.6 0.6 copy-start.8
  24.8 9.1 %collective-permute-start.2 = (bf16[2,144,256]{2,1,0:T(8,128)(2,1)}, bf16[2,144,256]{2,1,0:T(8,128)(2,1)S(1)}, u32[]{:S(2)}, u32[]{:S(2)}) collective-permute-start(bf16[2,144,256]{2,1,0:T(8,128)(2,1)} %get-tuple-element.18), channel_id=1, source_target_pairs={{0,8},{8,0},{16,24},{24,16},{1,9},{9,1},{17,25},{25,17},{2,10},{10... | collective-permute-start | bytes 442376 | tf_op jit(solution)/shard_map/ppermute | solution.py:251
  27.2 7.3 %collective-permute-start.3 = (bf16[2,144,256]{2,1,0:T(8,128)(2,1)}, bf16[2,144,256]{2,1,0:T(8,128)(2,1)S(1)}, u32[]{:S(2)}, u32[]{:S(2)}) collective-permute-start(bf16[2,144,256]{2,1,0:T(8,128)(2,1)} %get-tuple-element.19), channel_id=1, source_target_pairs={{0,16},{8,24},{16,0},{24,8},{1,17},{9,25},{17,1},{25,9},{2,18},{10... | collective-permute-start | bytes 442376 | tf_op jit(solution)/shard_map/ppermute | solution.py:251
  27.2 7.3 %collective-permute-start.4 = (bf16[2,144,256]{2,1,0:T(8,128)(2,1)}, bf16[2,144,256]{2,1,0:T(8,128)(2,1)S(1)}, u32[]{:S(2)}, u32[]{:S(2)}) collective-permute-start(bf16[2,144,256]{2,1,0:T(8,128)(2,1)} %get-tuple-element.20), channel_id=1, source_target_pairs={{0,24},{8,16},{16,8},{24,0},{1,25},{9,17},{17,9},{25,1},{2,26},{10... | collective-permute-start | bytes 442376 | tf_op jit(solution)/shard_map/ppermute | solution.py:251
  33.8 0.7 copy-start.3
  34.5 0.7 copy-start.4
  34.5 0.7 copy-start.5
  39.8 3.8 %copy-start.9 = (s32[64,2]{0,1:T(2,128)S(1)}, s32[64,2]{0,1:T(2,128)}, u32[]{:S(2)}) copy-start(s32[64,2]{0,1:T(2,128)} %param.36) | copy-start | bytes 1540
  39.8 40.0 %copy-start.1 = (bf16[64,2048]{1,0:T(8,128)(2,1)S(1)}, bf16[64,2048]{1,0:T(8,128)(2,1)}, u32[]{:S(2)}) copy-start(bf16[64,2048]{1,0:T(8,128)(2,1)} %param.19) | copy-start | bytes 786436
  39.8 41.2 %copy-start.6 = (f32[2048]{0:T(1024)S(1)}, f32[2048]{0:T(1024)}, u32[]{:S(2)}) copy-start(f32[2048]{0:T(1024)} %param.32) | copy-start | bytes 24580
  43.6 116.4 %all-gather.2.cloned.1.call-start = ((), (), s32[]{:S(2)}) async-start(), calls=%async_computation.5 | async-start | bytes 7077888 | tf_op jit(solution)/shard_map/all_gather | solution.py:350
  95.8 154.2 %reduce-scatter.5.cloned.1.call-start = ((), (), s32[]{:S(2)}) async-start(), calls=%async_computation.6 | async-start | bytes 7077888 | tf_op jit(solution)/shard_map/reduce_scatter | solution.py:358
  181.5 75.0 %copy-start.10 = (f32[64,2]{0,1:T(2,128)S(1)}, f32[64,2]{0,1:T(2,128)}, u32[]{:S(2)}) copy-start(f32[64,2]{0,1:T(2,128)} %param.37) | copy-start | bytes 1540
  181.5 88.4 %copy-start.2 = (bf16[64,2048]{1,0:T(8,128)(2,1)S(1)}, bf16[64,2048]{1,0:T(8,128)(2,1)}, u32[]{:S(2)}) copy-start(bf16[64,2048]{1,0:T(8,128)(2,1)} %reduce-scatter.3.cloned.1.call-done) | copy-start | bytes 786436
  252.9 12.7 %all-to-all-start.1 = ((bf16[96,2,2048]{2,1,0:T(2,128)(2,1)}), bf16[96,2,2048]{2,1,0:T(2,128)(2,1)S(1)}, u32[]{:S(2)}, u32[]{:S(2)}) async-start(bf16[96,2,2048]{2,1,0:T(2,128)(2,1)} %copy.49), calls=%async_computation.3 | async-start | bytes 1572864 | tf_op jit(solution)/shard_map/all_to_all | solution.py:366
Sparse Core Ops, SparseCore 0:
  43.7 36.1 reduce-scatter.2
  95.9 63.9 all-gather.1
  181.6 68.3 reduce-scatter.4
